TPU v7x, 32 devices: a whole 2x2x4 slice. The times are simulated.
32 devices in a mesh: sp: 4 (over y, x), tp: 8 (over z, core).
Axes of the slice: x: 2, y: 2, z: 4, core: 2. Of those that a mesh axis runs over, the one named last changes fastest.
Arguments:
- tokens: bfloat16 [8, 1536, 2048], P('tp', 'sp'), may hold values from -12 to 12
- norm_gain: float32 [2, 2048], replicated, may hold values from 0.1 to 1.9
- in_weight: bfloat16 [2, 2048, 512], P(None, 'sp', 'tp'), may hold values from -0.125 to 0.125
- down_weight: bfloat16 [2, 512, 2048], P(None, 'sp', 'tp'), may hold values from -0.25 to 0.25
- pool_gain: float32 [2, 512], replicated, may hold values from 0.1 to 1.9
Outputs:
- mixed: bfloat16 [8, 1536, 2048], P('tp', 'sp')
All inputs are finite; a program needn't handle non-finite values.
Results may differ from a plain program's by a relative error of at most 0.0061.
Values may be sent and summed in bfloat16 or wider, within the bound.
A program may use at most 64 MiB of HBM per device.

v0:
```python
import functools
import math

import jax
import jax.numpy as jnp
from jax import lax
from jax.experimental import pallas as pl
from jax.experimental.pallas import tpu as pltpu
from jax.sharding import PartitionSpec as P

GROUP = 64


EPS = 1e-06
WINDOWS = (2, 4, 8, 16)


def from_behind(block, axis, distance):
    devices = range(lax.axis_size(axis))
    route = [(i - distance, i) for i in devices if i - distance in devices]
    return lax.ppermute(block, axis, route)


def pool_rows(extended, first_pos, channel):
    sum_two = extended[1:] + extended[:-1]
    sum_four = sum_two[2:] + sum_two[:-2]
    sum_eight = sum_four[4:] + sum_four[:-4]
    sum_sixteen = sum_eight[8:] + sum_eight[:-8]
    count = extended.shape[0] - 15
    sums = (sum_two[-count:], sum_four[-count:], sum_eight[-count:], sum_sixteen)
    position = (first_pos + lax.iota(jnp.int32, count) + 1).astype(jnp.float32)
    which_one = channel // GROUP % 4
    result = jnp.zeros((count, extended.shape[1]), jnp.float32)
    for index, window in enumerate(WINDOWS):
        average = sums[index] / jnp.minimum(position, float(window))[:, None]
        result = jnp.where(which_one[None, :] == index, average, result)
    return result - extended[15:]


def local(tokens, norm_gain, in_weight, down_weight, pool_gain):
    stream = tokens[0]
    tok_rows = stream.shape[0]
    pool_cols = pool_gain.shape[1]
    first_pos = lax.axis_index("sp") * tok_rows
    channel = lax.iota(jnp.int32, pool_cols)
    for layer_index in range(in_weight.shape[0]):
        residual = stream.astype(jnp.float32)
        inverse_rms = lax.rsqrt(jnp.mean(residual * residual, axis=1, keepdims=True) + EPS)
        normed = (residual * inverse_rms * norm_gain[layer_index]).astype(jnp.bfloat16)
        layer_in, layer_down = (
            lax.all_gather(in_weight[layer_index], "tp", axis=1, tiled=True),
            lax.all_gather(down_weight[layer_index], "tp", axis=1, tiled=True),
        )
        pool_acc = jnp.dot(
            normed,
            lax.all_gather(layer_in, "sp", axis=0, tiled=True),
            preferred_element_type=jnp.float32,
        )
        pool_in = pool_acc.astype(jnp.bfloat16)
        before = from_behind(pool_in[tok_rows - 15 :], "sp", 1)
        extended = jnp.concatenate([before, pool_in], axis=0).astype(jnp.float32)
        trailing = pool_rows(extended, first_pos, channel)
        pooled = (trailing * pool_gain[layer_index]).astype(jnp.bfloat16)
        down = jnp.dot(
            pooled,
            lax.all_gather(layer_down, "sp", axis=0, tiled=True),
            preferred_element_type=jnp.float32,
        )
        stream = (residual + down).astype(jnp.bfloat16)
    return stream[None]


UNITS = ((False, 0, False), (True, 0, False), (True, 1, False), (False, 1, True))
MESH = pl.DeviceIdType.MESH


def mixer_kernel(
    n_z, rows_sp,
    tok_hbm, norm_gain, in_hbm, down_hbm, pool_gain, out_hbm,
    w_in, w_down, tok, normed, pool, pooled, halo,
    recv_sem, z_sem, a_sem, b_sem, d_sem, d_recv, h_send, h_recv, local_sem,
):
    n_s = 4
    s, t = lax.axis_index("sp"), lax.axis_index("tp")
    z, c = t // 2, t % 2
    y, x = s // 2, s % 2
    s_x, s_y = y * 2 + (1 - x), (1 - y) * 2 + x
    s_a, s_b, s_d = s_x + c * (s_y - s_x), s_y + c * (s_x - s_y), 3 - s
    partner = z * 2 + (1 - c)
    in_cols, in_rows = in_hbm.shape[1:]
    d_rows, d_cols = down_hbm.shape[1:]
    n_tok, width = tok.shape
    p_size = pool.shape[1]

    def unit(u, us, uz):
        is_in, layer, _ = UNITS[u]
        if is_in:
            col = pl.multiple_of((uz * 2 + c) * in_cols, in_cols)
            return w_in.at[layer, pl.ds(col, in_cols), pl.ds(pl.multiple_of(us * in_rows, in_rows), in_rows)]
        row = pl.multiple_of(us * d_rows, d_rows)
        return w_down.at[layer, pl.ds(row, d_rows), pl.ds(pl.multiple_of((uz * 2 + c) * d_cols, d_cols), d_cols)]

    def many(u, k):
        is_in, layer, _ = UNITS[u]
        if is_in:
            return w_in.at[layer, pl.ds(0, in_cols * k), pl.ds(0, in_rows * n_z)]
        return w_down.at[layer, pl.ds(0, d_rows // 2 * k), :]

    def few(u, k):
        is_in, layer, _ = UNITS[u]
        if is_in:
            return w_in.at[layer, pl.ds(0, in_cols * k), pl.ds(0, in_rows)]
        return w_down.at[layer, pl.ds(0, d_rows * k), pl.ds(0, d_cols)]

    def number(u, us, uz):
        return u * (n_s * n_z) + us * n_z + uz

    def to(u, us, uz, send, device_s, device_t):
        ref = unit(u, us, uz)
        return pltpu.make_async_remote_copy(
            ref, ref, send, recv_sem.at[number(u, us, uz)],
            device_id=(device_s, device_t), device_id_type=MESH)

    def to_up(u, us, uz):
        return to(u, us, uz, z_sem.at[((u * 2) * n_s + us) * n_z + uz], s, t + 2)

    def to_down(u, us, uz):
        return to(u, us, uz, z_sem.at[((u * 2 + 1) * n_s + us) * n_z + uz], s, t - 2)

    def to_a(u, uz):
        return to(u, s, uz, a_sem.at[u], s_a, t)

    def to_b(u, us, uz):
        return to(u, us, uz, b_sem.at[u], s_b, t)

    def to_partner(u, us, uz):
        ref = unit(u, us, uz)
        return pltpu.make_async_remote_copy(
            ref, ref, d_sem.at[u], d_recv.at[u], device_id=(s, partner), device_id_type=MESH)

    def arrive(u, us, uz):
        ref = unit(u, us, uz)
        pltpu.make_async_copy(ref, ref, recv_sem.at[number(u, us, uz)]).wait()

    def up(u, us, uz, finish=False):
        @pl.when(z < n_z - 1)
        def _():
            to_up(u, us, uz).wait_send() if finish else to_up(u, us, uz).start()

    def down(u, us, uz, finish=False):
        @pl.when(z > 0)
        def _():
            to_down(u, us, uz).wait_send() if finish else to_down(u, us, uz).start()

    def own(u):
        placed[u].wait()
        up(u, s, z)
        down(u, s, z)
        to_b(u, s, z).start()
        to_a(u, z).start()
        to_partner(u, s, z).start()

    def at_distance(d, body):
        if d == 0:
            body(z, True)
            return

        @pl.when(z - d >= 0)
        def _():
            body(z - d, True)

        @pl.when(z + d < n_z)
        def _():
            body(z + d, False)

    def places(u):
        return (s, s_a, s_b, s_d) if UNITS[u][2] else (s,)

    def along_z(u, d):
        def body(uz, from_below):
            for us in places(u):
                arrive(u, us, uz)
                up(u, us, uz) if from_below else down(u, us, uz)
                if not UNITS[u][2]:
                    to_b(u, us, uz).start()
                    to_a(u, uz).start()
                to_partner(u, us, uz).start()
        at_distance(d, body)

    def along_a(u, d):
        def body(uz, _):
            arrive(u, s_a, uz)
            to_b(u, s_a, uz).start()
            if UNITS[u][2]:
                up(u, s_a, uz)
                down(u, s_a, uz)
            to_partner(u, s_a, uz).start()
        at_distance(d, body)

    def along_b(u, d):
        def body(uz, _):
            for us in (s_b, s_d):
                arrive(u, us, uz)
                if UNITS[u][2]:
                    up(u, us, uz)
                    down(u, us, uz)
                to_partner(u, us, uz).start()
        at_distance(d, body)

    def ready(u):
        pltpu.make_async_copy(many(u, 4), many(u, 4), d_recv.at[u]).wait()

    def local_copy(src, dst, index):
        return pltpu.make_async_copy(src, dst, local_sem.at[index])

    barrier = pltpu.get_barrier_semaphore()

    def greet(device_s, device_t):
        pl.semaphore_signal(barrier, inc=1, device_id=(device_s, device_t), device_id_type=MESH)

    greet(s, partner)
    greet(s_x, t)
    greet(s_y, t)
    for cond, ds, dt in ((z > 0, s, t - 2), (z < n_z - 1, s, t + 2), (s > 0, s - 1, t), (s < n_s - 1, s + 1, t)):
        @pl.when(cond)
        def _():
            greet(ds, dt)

    placed = [
        local_copy((in_hbm if is_in else down_hbm).at[l], unit(u, s, z), u) for u, (is_in, l, _) in enumerate(UNITS)
    ]
    tok_in = local_copy(tok_hbm.at[0], tok, 4)
    for copy in placed:
        copy.start()
    tok_in.start()
    met = 3
    for cond in (z > 0, z < n_z - 1, s > 0, s < n_s - 1):
        met = met + jnp.where(cond, 1, 0)
    pl.semaphore_wait(barrier, met)

    def norm(layer):
        step = 32

        def body(i, carry):
            at = pl.ds(pl.multiple_of(i * step, step), step)
            value = tok[at, :].astype(jnp.float32)
            inverse = lax.rsqrt(jnp.mean(value * value, axis=1, keepdims=True) + EPS)
            normed[at, :] = (value * inverse * norm_gain[layer : layer + 1, :]).astype(jnp.bfloat16)
            return carry
        lax.fori_loop(0, n_tok // step, body, 0)

    def project_in(layer):
        tile = 256
        for j in range(p_size // tile):
            cols = pl.ds(j * tile, tile)
            pool[:, cols] = lax.dot_general(
                normed[...], w_in[layer, cols, :], (((1,), (1,)), ((), ())),
                preferred_element_type=jnp.float32).astype(jnp.bfloat16)

    def halo_copy(layer):
        return pltpu.make_async_remote_copy(
            pool.at[pl.ds(n_tok - 16, 16), :], halo.at[layer], h_send.at[layer], h_recv.at[layer],
            device_id=(s + 1, t), device_id_type=MESH)

    def send_halo(layer):
        @pl.when(s < n_s - 1)
        def _():
            halo_copy(layer).start()

    def pool_all(layer):
        lanes, head = 128, 128
        for start, size in ((head, n_tok - head), (0, head)):
            if start == 0:
                @pl.when(s > 0)
                def _():
                    halo_copy(layer).wait_recv()

                @pl.when(s == 0)
                def _():
                    halo[layer] = jnp.zeros(halo.shape[1:], halo.dtype)

            lane = lax.broadcasted_iota(jnp.int32, (size, lanes), 1)
            position = (s * n_tok + lax.broadcasted_iota(jnp.int32, (size, lanes), 0) + 1).astype(jnp.float32)
            for j in range(p_size // lanes):
                cols = pl.ds(j * lanes, lanes)
                if start == 0:
                    value = jnp.concatenate([halo[layer, :, cols], pool[:size, cols]], axis=0)
                else:
                    value = pool[start - 16 :, cols]
                value = value.astype(jnp.float32)
                sums, total, reach = {}, value, 1
                for window in WINDOWS:
                    total = total + pltpu.roll(total, reach, 0)
                    sums[window] = total
                    reach *= 2
                result = None
                for g in range(lanes // GROUP):
                    window = WINDOWS[(j * lanes // GROUP + g) % 4]
                    if start == 0:
                        average = sums[window][16:] / jnp.minimum(position, float(window))
                    else:
                        average = sums[window][16:] * (1.0 / window)
                    result = average if result is None else jnp.where(lane < g * GROUP, result, average)
                result = (result - value[16:]) * pool_gain[layer : layer + 1, cols]
                pooled[start : start + size, cols] = result.astype(jnp.bfloat16)

        @pl.when(s < n_s - 1)
        def _():
            halo_copy(layer).wait_send()

    def project_down(layer, last):
        tile = 256

        def body(j, carry):
            cols = pl.ds(pl.multiple_of(j * tile, tile), tile)
            down = jnp.dot(pooled[...], w_down[layer, :, cols], preferred_element_type=jnp.float32)
            tok[:, cols] = (tok[:, cols].astype(jnp.float32) + down).astype(jnp.bfloat16)
            if last:
                pltpu.make_async_copy(tok.at[:, cols], out_hbm.at[0, :, cols], local_sem.at[5 + j]).start()
            return carry
        lax.fori_loop(0, width // tile, body, 0)
        if last:
            for j in range(width // tile):
                cols = pl.ds(j * tile, tile)
                pltpu.make_async_copy(tok.at[:, cols], out_hbm.at[0, :, cols], local_sem.at[5 + j]).wait()

    far = range(n_z)
    own(0)
    own(1)
    own(2)
    own(3)
    tok_in.wait()
    along_z(0, 1)
    along_z(1, 1)
    norm(0)
    along_a(0, 0)
    along_a(1, 0)
    along_a(3, 0)
    along_b(3, 0)
    along_z(0, 2)
    along_z(1, 2)
    along_a(0, 1)
    along_a(1, 1)
    along_z(2, 1)
    along_z(0, 3)
    along_z(1, 3)
    along_a(0, 2)
    along_a(1, 2)
    along_a(2, 0)
    along_z(3, 1)
    along_a(0, 3)
    along_a(1, 3)
    along_z(2, 2)
    along_a(2, 1)
    for d in far:
        along_b(0, d)
    for d in far:
        along_b(1, d)
    ready(0)
    ready(1)
    project_in(0)
    send_halo(0)
    along_z(2, 3)
    along_a(2, 2)
    along_z(3, 2)
    pool_all(0)
    along_a(2, 3)
    project_down(0, False)
    norm(1)
    along_z(3, 3)
    for d in far:
        along_b(2, d)
    ready(2)
    project_in(1)
    send_halo(1)
    pool_all(1)
    ready(3)
    project_down(1, True)

    for u, (_, _, z_last) in enumerate(UNITS):
        for ref, sem in (
            (few(u, 1) if z_last else many(u, 1), a_sem),
            (few(u, 2) if z_last else many(u, 2), b_sem),
            (many(u, 4), d_sem),
        ):
            pltpu.make_async_copy(ref, ref, sem.at[u]).wait()

        def body(uz, from_below):
            for us in places(u):
                up(u, us, uz, True) if from_below else down(u, us, uz, True)

        for us in places(u):
            up(u, us, z, True)
            down(u, us, z, True)
        for d in range(1, n_z):
            at_distance(d, body)


def fused(n_z, tokens, norm_gain, in_weight, down_weight, pool_gain):
    n_tok, width = tokens.shape[1:]
    p_size = pool_gain.shape[1]
    n_u = len(UNITS)
    any_spec, vmem = pl.BlockSpec(memory_space=pltpu.HBM), pl.BlockSpec(memory_space=pltpu.VMEM)
    dma = pltpu.SemaphoreType.DMA
    bf16 = jnp.bfloat16
    return pl.pallas_call(
        functools.partial(mixer_kernel, n_z, 4),
        out_shape=jax.ShapeDtypeStruct(tokens.shape, tokens.dtype),
        in_specs=[any_spec, vmem, any_spec, any_spec, vmem],
        out_specs=any_spec,
        scratch_shapes=[
            pltpu.VMEM((2, p_size, width), bf16),
            pltpu.VMEM((2, p_size, width), bf16),
            pltpu.VMEM((n_tok, width), bf16),
            pltpu.VMEM((n_tok, width), bf16),
            pltpu.VMEM((n_tok, p_size), bf16),
            pltpu.VMEM((n_tok, p_size), bf16),
            pltpu.VMEM((2, 16, p_size), bf16),
            dma((n_u * 4 * n_z,)),
            dma((n_u * 2 * 4 * n_z,)),
            dma((n_u,)),
            dma((n_u,)),
            dma((n_u,)),
            dma((n_u,)),
            dma((2,)),
            dma((2,)),
            dma((5 + width // 256,)),
        ],
        compiler_params=pltpu.CompilerParams(
            collective_id=0, has_side_effects=True, vmem_limit_bytes=67_043_328),
    )(tokens, norm_gain, jnp.swapaxes(in_weight, 1, 2), down_weight, pool_gain)


def fits(n_sp, n_tp, tokens, in_weight, down_weight):
    n_tok, width = tokens.shape[1:]
    layers, in_rows, in_cols = in_weight.shape
    d_rows, d_cols = down_weight.shape[1:]
    return (
        n_sp == 4 and n_tp % 2 == 0 and layers == 2 and tokens.shape[0] == 1
        and in_cols % 32 == 0 and d_cols % 128 == 0 and d_rows % 32 == 0 and in_rows % 128 == 0
        and n_tp * in_cols == 4 * d_rows
        and n_tok % 128 == 0 and n_tok > 128 and width % 256 == 0 and width * n_tok <= 2**20
    )


def solution(mesh):
    n_sp, n_tp = mesh.shape["sp"], mesh.shape["tp"]
    in_specs = (P("tp", "sp", None), P(), P(None, "sp", "tp"), P(None, "sp", "tp"), P())
    out_specs = P("tp", "sp", None)

    def per_device(tokens, norm_gain, in_weight, down_weight, pool_gain):
        if fits(n_sp, n_tp, tokens, in_weight, down_weight):
            return fused(n_tp // 2, tokens, norm_gain, in_weight, down_weight, pool_gain)
        return local(tokens, norm_gain, in_weight, down_weight, pool_gain)

    return jax.shard_map(per_device, mesh=mesh, in_specs=in_specs, out_specs=out_specs, check_vma=False)
```

profile of v0, /device:TPU:0, one launch (start us, length us, event | category | flops | bytes accessed | tf_op | source)
XLA Modules:
  0.0 55.3 jit_solution(8650306506307310146)
XLA Ops:
  0.0 52.6 %shard_map.55 = bf16[1,384,2048]{2,1,0:T(8,128)(2,1)} custom-call(bf16[1,384,2048]{2,1,0:T(8,128)(2,1)} %tok_hbm.1, f32[2,2048]{1,0:T(2,128)} %norm_gain.1, bf16[2,64,512]{2,1,0:T(8,128)(2,1)} %bitcast.1, bf16[2,128,256]{2,1,0:T(8,128)(2,1)} %down_hbm.1, f32[2,512]{1,0:T(2,128)} %pool_gain.1), custom_call_target="tpu_custom_call" | custom-call | tf_op jit(solution)/shard_map/pallas_call | solution.py:406
  52.6 2.7 %copy.7 = bf16[1,384,2048]{2,1,0:T(8,128)(2,1)} copy(bf16[1,384,2048]{2,1,0:T(8,128)(2,1)} %shard_map.55) | data formatting | bytes 3145728
where the time goes:
time: 55.6 us; the launch traced here: 55.3 us
  Pallas kernels  52.6 us (95%)
  local copies, waits for them, and re-layouts  2.73 us (5%)
    pallas_call x1, Pallas kernels, fused(): pl.pallas_call(functools.partial(mixer_kernel, n_z, 4), out_shape=jax.Sha...  52.6 us
    unnamed x1, local copies, waits for them, and re-layouts  2.73 us

commit v1 on v0

--- a/solution.py
+++ b/solution.py
@@ -76,11 +76,12 @@
 
 def mixer_kernel(
     n_z, rows_sp,
-    tok_hbm, norm_gain, in_hbm, down_hbm, pool_gain, out_hbm,
-    w_in, w_down, tok, normed, pool, pooled, halo,
+    tok_hbm, norm_gain, in_hbm, down_hbm, pool_gain, out,
+    w_in, w_down, normed, pool, pooled, halo,
     recv_sem, z_sem, a_sem, b_sem, d_sem, d_recv, h_send, h_recv, local_sem,
 ):
     n_s = 4
+    tok = out.at[0]
     s, t = lax.axis_index("sp"), lax.axis_index("tp")
     z, c = t // 2, t % 2
     y, x = s // 2, s % 2
@@ -315,14 +316,8 @@
             cols = pl.ds(pl.multiple_of(j * tile, tile), tile)
             down = jnp.dot(pooled[...], w_down[layer, :, cols], preferred_element_type=jnp.float32)
             tok[:, cols] = (tok[:, cols].astype(jnp.float32) + down).astype(jnp.bfloat16)
-            if last:
-                pltpu.make_async_copy(tok.at[:, cols], out_hbm.at[0, :, cols], local_sem.at[5 + j]).start()
             return carry
         lax.fori_loop(0, width // tile, body, 0)
-        if last:
-            for j in range(width // tile):
-                cols = pl.ds(j * tile, tile)
-                pltpu.make_async_copy(tok.at[:, cols], out_hbm.at[0, :, cols], local_sem.at[5 + j]).wait()
 
     far = range(n_z)
     own(0)
@@ -405,13 +400,12 @@
     bf16 = jnp.bfloat16
     return pl.pallas_call(
         functools.partial(mixer_kernel, n_z, 4),
-        out_shape=jax.ShapeDtypeStruct(tokens.shape, tokens.dtype),
+        out_shape=pltpu.VMEM(tokens.shape, tokens.dtype),
         in_specs=[any_spec, vmem, any_spec, any_spec, vmem],
-        out_specs=any_spec,
+        out_specs=vmem,
         scratch_shapes=[
             pltpu.VMEM((2, p_size, width), bf16),
             pltpu.VMEM((2, p_size, width), bf16),
-            pltpu.VMEM((n_tok, width), bf16),
             pltpu.VMEM((n_tok, width), bf16),
             pltpu.VMEM((n_tok, p_size), bf16),
             pltpu.VMEM((n_tok, p_size), bf16),
@@ -424,10 +418,10 @@
             dma((n_u,)),
             dma((2,)),
             dma((2,)),
-            dma((5 + width // 256,)),
+            dma((5,)),
         ],
         compiler_params=pltpu.CompilerParams(
-            collective_id=0, has_side_effects=True, vmem_limit_bytes=67_043_328),
+            collective_id=0, has_side_effects=True, vmem_limit_bytes=67_043_328 - 2 * n_tok * width),
     )(tokens, norm_gain, jnp.swapaxes(in_weight, 1, 2), down_weight, pool_gain)
 
 

time: 55.6 us -> 53.3 us (0.959)
  local copies, waits for them, and re-layouts: 2.73 us -> 1.15 us
  Pallas kernels: 52.6 us -> 51.9 us
    unnamed x1, local copies, waits for them, and re-layouts: 2.73 us -> 1.15 us
    pallas_call x1, Pallas kernels: 52.6 us -> 51.9 us  [fused(): pl.pallas_call(functools.partial(mixer_kernel, n_z, 4), out_shape=pltpu.V...]
where the time goes in v1:
time: 53.3 us; the launch traced here: 53 us
  Pallas kernels  51.9 us (97%)
  local copies, waits for them, and re-layouts  1.15 us (2%)
    pallas_call x1, Pallas kernels, fused(): pl.pallas_call(functools.partial(mixer_kernel, n_z, 4), out_shape=pltpu.V...  51.9 us
    unnamed x1, local copies, waits for them, and re-layouts  1.15 us

profile of v1, /device:TPU:0, one launch (start us, length us, event | category | flops | bytes accessed | tf_op | source)
XLA Modules:
  0.0 53.0 jit_solution(12717253583279769317)
XLA Ops:
  0.0 51.9 %shard_map.55 = bf16[1,384,2048]{2,1,0:T(8,128)(2,1)S(1)} custom-call(bf16[1,384,2048]{2,1,0:T(8,128)(2,1)} %tok_hbm.1, f32[2,2048]{1,0:T(2,128)} %norm_gain.1, bf16[2,64,512]{2,1,0:T(8,128)(2,1)} %bitcast.1, bf16[2,128,256]{2,1,0:T(8,128)(2,1)} %down_hbm.1, f32[2,512]{1,0:T(2,128)} %pool_gain.1), custom_call_target="tpu_custom_call" | custom-call | tf_op jit(solution)/shard_map/pallas_call | solution.py:401
  51.9 1.1 %copy.7 = bf16[1,384,2048]{2,1,0:T(8,128)(2,1)} copy(bf16[1,384,2048]{2,1,0:T(8,128)(2,1)S(1)} %shard_map.55) | data formatting | bytes 3145728
